TPU v7x, 256 devices: a whole 4x4x8 slice. The times are simulated.
256 devices in a mesh: sp: 64 (over z, x, core), tp: 4 (over y).
Axes of the slice: x: 4, y: 4, z: 8, core: 2. Of those that a mesh axis runs over, the one named last changes fastest.
Arguments:
- conv_in: bfloat16 [49152, 1024], P('sp', 'tp'), may hold values from -6 to 6
- conv_pre: bfloat16 [49152, 1024], P('sp', 'tp'), may hold values from -6 to 6
- conv_post: bfloat16 [49152, 1024], P('sp', 'tp'), may hold values from -6 to 6
- taps: float32 [3, 1024], P(None, 'tp'), may hold values from -3 to 3
- out_proj: bfloat16 [1024, 2048], P('tp'), may hold values from -0.1875 to 0.1875
- stream: bfloat16 [49152, 2048], P(('sp', 'tp')), may hold values from -6 to 6
- norm_gain: float32 [2048], replicated, may hold values from 0.1 to 1.9
- routes: int32 [49152, 2], P(('sp', 'tp')), may hold values from 0 to 63, all different within a row; in each aligned block of 192 rows (0 to 191, 192 to 383, ...) at most 8 rows name the same one
- route_weight: float32 [49152, 2], P(('sp', 'tp')), may hold values from 0.1 to 1
- gate_w: bfloat16 [64, 2048, 2048], P('sp', None, 'tp'), may hold values from -0.52734375 to 0.52734375
- up_w: bfloat16 [64, 2048, 2048], P('sp', None, 'tp'), may hold values from -0.52734375 to 0.52734375
- down_w: bfloat16 [64, 2048, 2048], P('sp', 'tp'), may hold values from -0.013244629 to 0.013244629
Outputs:
- output: bfloat16 [49152, 2048], P(('sp', 'tp'))
Inputs may be any that keep to these rules, and one draw needn't show every extreme that they name: `routes`: each row names 2 different experts. In each aligned block of 192 rows no expert is named more than 8 times, a bound that some block reaches.
All inputs are finite; a program needn't handle non-finite values.
Results may differ from a plain program's by a relative error of at most 0.015.
Values may be sent and summed in bfloat16 or wider, within the bound.
A program may use at most 128 MiB of HBM per device.

v0:
```python
import jax
import jax.numpy as jnp
from jax import lax
from jax.sharding import PartitionSpec as P

EPSILON = 1e-05
LIMIT = 7.0
ALPHA = 1.702
CAP = 8


def with_halo(x, axis):
    count, length = (lax.axis_size(axis), x.shape[0])
    up = [(i, (i + 1) % count) for i in range(count - 1)]
    down = [(j, i) for i, j in up]
    before = lax.ppermute(x[length - 1 :], axis, up)
    after = lax.ppermute(x[:1], axis, down)
    return jnp.concatenate([before, x, after], axis=0)


def clamped_unit(gate_pre, up_pre):
    gated = jnp.minimum(gate_pre, LIMIT)
    upward = jnp.clip(up_pre, -LIMIT, LIMIT)
    return (upward + 1.0) * gated * jax.nn.sigmoid(ALPHA * gated)


def local(
    conv_in,
    conv_pre,
    conv_post,
    taps,
    out_proj,
    stream,
    norm_gain,
    routes,
    route_weight,
    gate_w,
    up_w,
    down_w,
):
    product = conv_pre.astype(jnp.float32) * conv_in.astype(jnp.float32)
    padded = with_halo(product.astype(jnp.bfloat16), "sp").astype(product.dtype)
    convolved = taps[0] * padded[:-2] + taps[1] * padded[1:-1] + taps[2] * padded[2:]
    mixed = (conv_post.astype(jnp.float32) * convolved).astype(jnp.bfloat16)
    own_rows, width = stream.shape
    part = jnp.dot(mixed, out_proj, preferred_element_type=jnp.float32).astype(jnp.bfloat16)
    part = part.reshape(lax.axis_size("tp"), own_rows, width)
    branch = lax.all_to_all(part, "tp", split_axis=0, concat_axis=0, tiled=True)
    branch = branch.astype(jnp.float32).sum(axis=0)
    resid = (stream.astype(jnp.float32) + branch).astype(jnp.bfloat16)
    resid_f = resid.astype(jnp.float32)
    scale = lax.rsqrt(jnp.mean(resid_f * resid_f, axis=-1, keepdims=True) + EPSILON)
    normed = (resid_f * scale * norm_gain).astype(jnp.bfloat16)
    experts = lax.axis_size("sp")
    top = routes.shape[1]
    flat = routes.reshape(-1)
    onehot = (flat[:, None] == jnp.arange(experts, dtype=jnp.int32)[None, :]).astype(jnp.bfloat16)
    entry = jnp.arange(own_rows * top, dtype=jnp.int32)
    earlier = (entry[None, :] < entry[:, None]).astype(jnp.bfloat16)
    counts = jnp.dot(earlier, onehot, preferred_element_type=jnp.float32)
    rank = jnp.sum(counts * onehot.astype(jnp.float32), axis=1).astype(jnp.int32)
    slots = experts * CAP
    target = (flat * CAP + rank).reshape(own_rows, top)
    ids = jnp.arange(slots, dtype=jnp.int32)[None, None, :]
    chosen = target[:, :, None] == ids
    pick = chosen.any(axis=1).astype(jnp.bfloat16)
    outgoing = lax.dot_general(
        pick, normed, (((0,), (0,)), ((), ())), preferred_element_type=jnp.float32
    ).astype(jnp.bfloat16)
    outgoing = outgoing.reshape(experts, CAP, width)
    done = []
    for k in range(2):
        group = outgoing[:, k * 4 : (k + 1) * 4]
        arrived = lax.all_to_all(group, "sp", split_axis=0, concat_axis=0, tiled=True)
        rows = lax.all_gather(arrived.reshape(-1, width), "tp", axis=0, tiled=True)
        gate_pre = jnp.dot(rows, gate_w[0], preferred_element_type=jnp.float32)
        up_pre = jnp.dot(rows, up_w[0], preferred_element_type=jnp.float32)
        active = clamped_unit(gate_pre, up_pre).astype(jnp.bfloat16)
        partial = jnp.dot(active, down_w[0], preferred_element_type=jnp.float32)
        summed = lax.psum_scatter(
            partial.astype(jnp.bfloat16), "tp", scatter_dimension=0, tiled=True
        )
        done.append(
            lax.all_to_all(
                summed.reshape(experts, 4, width), "sp", split_axis=0, concat_axis=0, tiled=True
            )
        )
    spread = jnp.sum(jnp.where(chosen, route_weight[:, :, None], 0.0), axis=1)
    total = resid.astype(jnp.float32)
    for k in range(2):
        share = spread.reshape(own_rows, experts, CAP)[:, :, k * 4 : (k + 1) * 4]
        share = share.reshape(own_rows, -1)
        high = share.astype(jnp.bfloat16)
        low = (share - high.astype(jnp.float32)).astype(jnp.bfloat16)
        back = done[k].reshape(-1, width)
        total = total + jnp.dot(high, back, preferred_element_type=jnp.float32)
        total = total + jnp.dot(low, back, preferred_element_type=jnp.float32)
    return total.astype(jnp.bfloat16)


def solution(mesh):
    placed = (
        P("sp", "tp"),
        P("sp", "tp"),
        P("sp", "tp"),
        P(None, "tp"),
        P("tp", None),
        P(("sp", "tp"), None),
        P(),
        P(("sp", "tp"), None),
        P(("sp", "tp"), None),
        P("sp", None, "tp"),
        P("sp", None, "tp"),
        P("sp", "tp", None),
    )
    return jax.shard_map(
        local, mesh=mesh, in_specs=placed, out_specs=P(("sp", "tp"), None), check_vma=False
    )
```

profile of v0, /device:TPU:1, one launch (start us, length us, event | category | flops | bytes accessed | tf_op | source)
XLA Modules:
  0.0 367.3 jit_solution(12065180576500988461)
XLA Ops:
  6.5 1.4 multiply_convert_fusion.2
  7.9 4.5 %collective-permute-start = (bf16[1,256]{1,0:T(2,128)(2,1)S(1)}, bf16[1,256]{1,0:T(2,128)(2,1)S(1)}, u32[]{:S(2)}, u32[]{:S(2)}) collective-permute-start(bf16[1,256]{1,0:T(2,128)(2,1)S(1)} %get-tuple-element.11), channel_id=1, source_target_pairs={{0,4},{4,8},{8,12},{12,16},{16,20},{20,24},{24,28},{28,32},{32,36}... | collective-permute-start | bytes 1544 | tf_op jit(solution)/shard_map/ppermute | solution.py:16
  12.4 1.9 collective-permute-start.1
  14.4 0.8 fusion.57
  15.2 2.2 collective-permute-done.1
  17.3 0.1 maximum_convert_fusion
  17.4 2.8 convolution_convert_fusion.2
  20.2 4.8 %all-to-all-start = ((bf16[4,192,2048]{2,1,0:T(8,128)(2,1)}), bf16[4,192,2048]{2,1,0:T(8,128)(2,1)}, u32[]{:S(2)}, u32[]{:S(2)}) async-start(bf16[4,192,2048]{2,1,0:T(8,128)(2,1)} %bitcast.54), calls=%async_computation | async-start | bytes 6291456 | tf_op jit(solution)/shard_map/all_to_all | solution.py:48
  25.1 0.1 copy.46
  25.2 0.1 eq.28
  25.4 0.2 fusion.23
  25.6 0.1 convert_element_type.111
  25.8 0.1 copy.47
  25.8 0.1 fusion.39
  26.0 35.6 %all-to-all-done = bf16[4,192,2048]{2,1,0:T(8,128)(2,1)} async-done(((bf16[4,192,2048]{2,1,0:T(8,128)(2,1)}), bf16[4,192,2048]{2,1,0:T(8,128)(2,1)}, u32[]{:S(2)}, u32[]{:S(2)}) %all-to-all-start) | async-done | bytes 3145760 | tf_op jit(solution)/shard_map/all_to_all | solution.py:48
  61.6 2.7 convert_reduce_fusion
  64.3 0.3 fusion.20
  64.6 0.9 copy-done.3
  65.5 0.8 fusion
  66.3 2.1 fusion.54
  68.5 40.6 %all_to_all.25 = bf16[64,4,2048]{2,1,0:T(4,128)(2,1)S(1)} all-to-all(bf16[64,4,2048]{2,1,0:T(4,128)(2,1)S(1)} %get-tuple-element.8), channel_id=1, replica_groups=mesh['sp'=64,'tp'=4] {'sp'}, dimensions={0} | all-to-all | bytes 2097152 | tf_op jit(solution)/shard_map/all_to_all | solution.py:74
  109.1 1.2 reshape.55
  110.3 34.4 %all_to_all.26 = bf16[64,4,2048]{2,1,0:T(4,128)(2,1)S(1)} all-to-all(bf16[64,4,2048]{2,1,0:T(4,128)(2,1)} %get-tuple-element.7), channel_id=1, replica_groups=mesh['sp'=64,'tp'=4] {'sp'}, dimensions={0} | all-to-all | bytes 2097152 | tf_op jit(solution)/shard_map/all_to_all | solution.py:74
  144.8 1.1 reshape.53
  145.9 0.2 reduce-scatter.5.cloned.1.call-start
  146.1 9.9 %all-gather.5.cloned.1.call-done = bf16[1024,2048]{1,0:T(8,128)(2,1)} async-done(((bf16[256,2048]{1,0:T(8,128)(2,1)}), bf16[1024,2048]{1,0:T(8,128)(2,1)}) %all-gather.5.cloned.1.call-update) | async-done | bytes 4194320 | tf_op jit(solution)/shard_map/all_gather | solution.py:75
  156.1 6.6 %fusion.12 = f32[1024,512]{1,0:T(8,128)} fusion(bf16[1024,2048]{1,0:T(8,128)(2,1)} %all-gather.5.cloned.1.call-done, bf16[1,2048,512]{2,1,0:T(8,128)(2,1)} %param.22), kind=kOutput, calls=%fused_computation.23 | convolution fusion | flops 2147483648 | bytes 8388608 | tf_op jit(solution)/shard_map/dot_general | solution.py:77
  162.7 10.3 %convolution_convert_fusion = bf16[1024,2048]{1,0:T(8,128)(2,1)} fusion(bf16[1,512,2048]{2,1,0:T(8,128)(2,1)S(1)} %copy-done, f32[1024,512]{1,0:T(8,128)} %fusion.12, bf16[1024,2048]{1,0:T(8,128)(2,1)} %all-gather.5.cloned.1.call-done, bf16[1,2048,512]{2,1,0:T(8,128)(2,1)} %param.21), kind=kOutput, calls=%fused_computation.1 | convolution fusion | flops 4302307328 | bytes 14680064 | tf_op jit(solution)/shard_map/dot_general | solution.py:79
  173.0 0.0 reduce-scatter.3.cloned.1.call-start
  173.0 36.0 %all-gather.3.cloned.1.call-done = bf16[1024,2048]{1,0:T(8,128)(2,1)} async-done(((bf16[256,2048]{1,0:T(8,128)(2,1)}), bf16[1024,2048]{1,0:T(8,128)(2,1)}) %all-gather.3.cloned.1.call-update) | async-done | bytes 4194320 | tf_op jit(solution)/shard_map/all_gather | solution.py:75
  209.1 6.5 %fusion.14 = f32[1024,512]{1,0:T(8,128)} fusion(bf16[1024,2048]{1,0:T(8,128)(2,1)} %all-gather.3.cloned.1.call-done, bf16[1,2048,512]{2,1,0:T(8,128)(2,1)} %param.22), kind=kOutput, calls=%fused_computation.25 | convolution fusion | flops 2147483648 | bytes 8388608 | tf_op jit(solution)/shard_map/dot_general | solution.py:77
  215.6 10.3 %convolution_convert_fusion.1 = bf16[1024,2048]{1,0:T(8,128)(2,1)} fusion(bf16[1,512,2048]{2,1,0:T(8,128)(2,1)S(1)} %copy-done, f32[1024,512]{1,0:T(8,128)} %fusion.14, bf16[1024,2048]{1,0:T(8,128)(2,1)} %all-gather.3.cloned.1.call-done, bf16[1,2048,512]{2,1,0:T(8,128)(2,1)} %param.21), kind=kOutput, calls=%fused_computation.2 | convolution fusion | flops 4302307328 | bytes 14680064 | tf_op jit(solution)/shard_map/dot_general | solution.py:79
  225.9 35.6 %reduce-scatter.5.cloned.1.call-done = bf16[256,2048]{1,0:T(8,128)(2,1)} async-done(((bf16[1024,2048]{1,0:T(8,128)(2,1)}), bf16[256,2048]{1,0:T(8,128)(2,1)}) %reduce-scatter.5.cloned.1.call-update) | async-done | bytes 1048592 | tf_op jit(solution)/shard_map/reduce_scatter | solution.py:80
  261.5 2.2 reshape.56
  263.7 10.7 %all-to-all-start.4 = ((bf16[64,4,2048]{2,1,0:T(4,128)(2,1)}), bf16[64,4,2048]{2,1,0:T(4,128)(2,1)S(1)}, u32[]{:S(2)}, u32[]{:S(2)}) async-start(bf16[64,4,2048]{2,1,0:T(4,128)(2,1)} %reshape.56), calls=%async_computation.6 | async-start | bytes 2097152 | tf_op jit(solution)/shard_map/all_to_all | solution.py:84
  274.5 38.6 %reduce-scatter.3.cloned.1.call-done = bf16[256,2048]{1,0:T(8,128)(2,1)} async-done(((bf16[1024,2048]{1,0:T(8,128)(2,1)}), bf16[256,2048]{1,0:T(8,128)(2,1)}) %reduce-scatter.3.cloned.1.call-update) | async-done | bytes 1048592 | tf_op jit(solution)/shard_map/reduce_scatter | solution.py:80
  313.1 2.3 reshape.54
  315.4 1.0 copy-done.1
  316.4 10.7 %all-to-all-start.2 = ((bf16[64,4,2048]{2,1,0:T(4,128)(2,1)}), bf16[64,4,2048]{2,1,0:T(4,128)(2,1)S(1)}, u32[]{:S(2)}, u32[]{:S(2)}) async-start(bf16[64,4,2048]{2,1,0:T(4,128)(2,1)} %reshape.54), calls=%async_computation.3 | async-start | bytes 2097152 | tf_op jit(solution)/shard_map/all_to_all | solution.py:84
  327.1 0.2 select_reduce_fusion
  327.3 1.0 copy.48
  328.3 1.4 fusion.55
  329.7 3.8 %convolution_bitcast_fusion.1 = f32[192,2048]{1,0:T(8,128)} fusion(bf16[64,4,2048]{2,1,0:T(4,128)(2,1)} %copy-done.1, f32[192,64,4]{0,2,1:T(4,128)S(1)} %get-tuple-element.10), kind=kOutput, calls=%fused_computation.7 | convolution fusion | flops 201326592 | bytes 2818048 | tf_op jit(solution)/shard_map/dot_general | solution.py:96
  333.5 2.5 convolution_bitcast_fusion
  336.0 19.3 %all-to-all-done.2 = bf16[64,4,2048]{2,1,0:T(4,128)(2,1)S(1)} async-done(((bf16[64,4,2048]{2,1,0:T(4,128)(2,1)}), bf16[64,4,2048]{2,1,0:T(4,128)(2,1)S(1)}, u32[]{:S(2)}, u32[]{:S(2)}) %all-to-all-start.2) | async-done | bytes 1048608 | tf_op jit(solution)/shard_map/all_to_all | solution.py:84
  355.3 1.4 convolution_bitcast_fusion.2
  356.7 0.3 copy-done.5
  356.9 3.9 %fusion.5 = bf16[192,2048]{1,0:T(8,128)(2,1)} fusion(f32[192,2048]{1,0:T(8,128)} %convolution_bitcast_fusion, f32[192,2048]{1,0:T(8,128)S(1)} %copy-done.5, f32[192,2048]{1,0:T(8,128)S(1)} %convolution_bitcast_fusion.2, bf16[192,2048]{1,0:T(8,128)(2,1)S(1)} %copy-done.4, bf16[64,4,2048]{2,1,0:T(4,128)(2,1)S(1)} %all-to-all-done.2, ...), kind=kOutput, calls=%fused_computation.14 | convolution fusion | flops 203685888 | bytes 7536640 | tf_op jit(solution)/shard_map/dot_general | solution.py:96
  (33 shorter events, 0.2 us)
Async XLA Ops:
  6.5 156.1 %copy-start = (bf16[1,512,2048]{2,1,0:T(8,128)(2,1)S(1)}, bf16[1,512,2048]{2,1,0:T(8,128)(2,1)}, u32[]{:S(2)}) copy-start(bf16[1,512,2048]{2,1,0:T(8,128)(2,1)} %param.23) | copy-start | bytes 6291460
  6.5 10.9 %copy-start.8 = (bf16[768,256]{1,0:T(8,128)(2,1)S(1)}, bf16[768,256]{1,0:T(8,128)(2,1)}, u32[]{:S(2)}) copy-start(bf16[768,256]{1,0:T(8,128)(2,1)} %param.14) | copy-start | bytes 1179652
  6.5 10.9 %copy-start.6 = (bf16[256,2048]{1,0:T(8,128)(2,1)S(1)}, bf16[256,2048]{1,0:T(8,128)(2,1)}, u32[]{:S(2)}) copy-start(bf16[256,2048]{1,0:T(8,128)(2,1)} %param.16) | copy-start | bytes 3145732
  7.9 7.2 %collective-permute-start = (bf16[1,256]{1,0:T(2,128)(2,1)S(1)}, bf16[1,256]{1,0:T(2,128)(2,1)S(1)}, u32[]{:S(2)}, u32[]{:S(2)}) collective-permute-start(bf16[1,256]{1,0:T(2,128)(2,1)S(1)} %get-tuple-element.11), channel_id=1, source_target_pairs={{0,4},{4,8},{8,12},{12,16},{16,20},{20,24},{24,28},{28,32},{32,36}... | collective-permute-start | bytes 1544 | tf_op jit(solution)/shard_map/ppermute | solution.py:16
  12.4 4.9 %collective-permute-start.1 = (bf16[1,256]{1,0:T(2,128)(2,1)S(1)}, bf16[1,256]{1,0:T(2,128)(2,1)S(1)}, u32[]{:S(2)}, u32[]{:S(2)}) collective-permute-start(bf16[1,256]{1,0:T(2,128)(2,1)S(1)} %get-tuple-element.12), channel_id=1, source_target_pairs={{4,0},{8,4},{12,8},{16,12},{20,16},{24,20},{28,24},{32,28},{36,32}... | collective-permute-start | bytes 1544 | tf_op jit(solution)/shard_map/ppermute | solution.py:17
  20.2 4.9 %copy-start.10 = (s32[192,2]{0,1:T(2,128)S(1)}, s32[192,2]{0,1:T(2,128)}, u32[]{:S(2)}) copy-start(s32[192,2]{0,1:T(2,128)} %param.19) | copy-start | bytes 4612
  20.2 41.3 %all-to-all-start = ((bf16[4,192,2048]{2,1,0:T(8,128)(2,1)}), bf16[4,192,2048]{2,1,0:T(8,128)(2,1)}, u32[]{:S(2)}, u32[]{:S(2)}) async-start(bf16[4,192,2048]{2,1,0:T(8,128)(2,1)} %bitcast.54), calls=%async_computation | async-start | bytes 6291456 | tf_op jit(solution)/shard_map/all_to_all | solution.py:48
  25.0 131.0 %all-gather.5.cloned.1.call-start = ((), (), s32[]{:S(2)}) async-start(), calls=%async_computation.9 | async-start | bytes 5242880 | tf_op jit(solution)/shard_map/all_gather | solution.py:75
  26.0 38.3 %copy-start.7 = (bf16[192,2048]{1,0:T(8,128)(2,1)S(1)}, bf16[192,2048]{1,0:T(8,128)(2,1)}, u32[]{:S(2)}) copy-start(bf16[192,2048]{1,0:T(8,128)(2,1)} %param.17) | copy-start | bytes 2359300
  64.3 1.2 copy-start.9
  64.6 0.9 copy-start.3
  110.3 98.8 %all-gather.3.cloned.1.call-start = ((), (), s32[]{:S(2)}) async-start(), calls=%async_computation.7 | async-start | bytes 5242880 | tf_op jit(solution)/shard_map/all_gather | solution.py:75
  145.9 115.6 %reduce-scatter.5.cloned.1.call-start = ((), (), s32[]{:S(2)}) async-start(), calls=%async_computation.10 | async-start | bytes 5242880 | tf_op jit(solution)/shard_map/reduce_scatter | solution.py:80
  173.0 140.1 %reduce-scatter.3.cloned.1.call-start = ((), (), s32[]{:S(2)}) async-start(), calls=%async_computation.8 | async-start | bytes 5242880 | tf_op jit(solution)/shard_map/reduce_scatter | solution.py:80
  263.7 51.6 %all-to-all-start.4 = ((bf16[64,4,2048]{2,1,0:T(4,128)(2,1)}), bf16[64,4,2048]{2,1,0:T(4,128)(2,1)S(1)}, u32[]{:S(2)}, u32[]{:S(2)}) async-start(bf16[64,4,2048]{2,1,0:T(4,128)(2,1)} %reshape.56), calls=%async_computation.6 | async-start | bytes 2097152 | tf_op jit(solution)/shard_map/all_to_all | solution.py:84
  274.5 52.6 %copy-start.11 = (f32[192,2]{0,1:T(2,128)S(1)}, f32[192,2]{0,1:T(2,128)}, u32[]{:S(2)}) copy-start(f32[192,2]{0,1:T(2,128)} %param.20) | copy-start | bytes 4612
  315.4 1.0 copy-start.1
  316.4 38.9 %all-to-all-start.2 = ((bf16[64,4,2048]{2,1,0:T(4,128)(2,1)}), bf16[64,4,2048]{2,1,0:T(4,128)(2,1)S(1)}, u32[]{:S(2)}, u32[]{:S(2)}) async-start(bf16[64,4,2048]{2,1,0:T(4,128)(2,1)} %reshape.54), calls=%async_computation.3 | async-start | bytes 2097152 | tf_op jit(solution)/shard_map/all_to_all | solution.py:84
  328.3 5.2 %copy-start.2 = (bf16[64,4,2048]{2,1,0:T(4,128)(2,1)S(1)}, bf16[64,4,2048]{2,1,0:T(4,128)(2,1)}, u32[]{:S(2)}) copy-start(bf16[64,4,2048]{2,1,0:T(4,128)(2,1)} %copy-done.1) | copy-start | bytes 3145732
  355.3 1.4 copy-start.4
  355.3 1.7 copy-start.5
Sparse Core Ops, SparseCore 0:
  110.4 45.6 all-gather.4
  157.9 51.1 all-gather.2
  211.6 49.8 reduce-scatter.4
  263.9 49.1 reduce-scatter.2
where the time goes:
time: 368 us; the launch traced here: 367 us
  waiting for transfers between devices  177 us (48%)
  blocking collectives  75 us (20%)
  matrix products  49.1 us (13%)
  starting transfers between devices  33 us (9%)
  local copies, waits for them, and re-layouts  14.8 us (4%)
  between operations  13.4 us (4%)
  other arithmetic  4.81 us (1%)
    all_to_all x2, blocking collectives, local(): lax.all_to_all(group, 'sp', split_axis=0, concat_axis=0, tiled=True)  75 us
    reduce_scatter x2, waiting for transfers between devices, local(): lax.psum_scatter(partial.astype(jnp.bfloat16), 'tp', scatter_dimension=0,...  74.2 us
    all_gather x2, waiting for transfers between devices, local(): rows = lax.all_gather(arrived.reshape(-1, width), 'tp', axis=0, tiled=True)  46 us
    all_to_all x1, waiting for transfers between devices, local(): branch = lax.all_to_all(part, 'tp', split_axis=0, concat_axis=0, tiled=True)  35.6 us
    all_to_all x2, starting transfers between devices, local(): lax.all_to_all(summed.reshape(experts, 4, width), 'sp', split_axis=0, con...  21.4 us
    dot_general x2, matrix products, local(): partial = jnp.dot(active, down_w[0], preferred_element_type=jnp.float32)  20.6 us
    all_to_all x2, waiting for transfers between devices, local(): lax.all_to_all(summed.reshape(experts, 4, width), 'sp', split_axis=0, con...  19.3 us
    dot_general x2, matrix products, local(): up_pre = jnp.dot(rows, up_w[0], preferred_element_type=jnp.float32)  13.1 us
  transfers between devices with their start and end apart: 9, of which 7 were waited for; matrix products, arithmetic and copies ran while one was open for 14% of the time, Pallas kernels for 0%

commit v1 on v0

--- a/solution.py
+++ b/solution.py
@@ -1,3 +1,4 @@
+import functools
 import jax
 import jax.numpy as jnp
 from jax import lax
@@ -7,6 +8,32 @@
 LIMIT = 7.0
 ALPHA = 1.702
 CAP = 8
+
+
+def settle_array_by_axis(m, chip_axis):
+    fresh = lax.axis_size(chip_axis)
+    d_next = lax.axis_index(chip_axis)
+    y_new, current_value, z2 = (fresh, d_next, m.shape[0])
+    store = [(ix, (ix + 1) % y_new) for ix in range(y_new)]
+    all_rows = [(ix, (ix - 1) % y_new) for ix in range(y_new)]
+    local_now = jnp.zeros((*m.shape[:0], y_new * z2, *m.shape[1:]), m.dtype)
+    local_now = lax.dynamic_update_slice_in_dim(local_now, m, current_value * z2, axis=0)
+    side_arr = extra = m
+    small = y_new // 2
+    for k0 in tuple(range(1, small + 1)):
+        side_arr = lax.ppermute(side_arr, axis_name=chip_axis, perm=store)
+        local_now = lax.dynamic_update_slice_in_dim(
+            local_now, side_arr, (current_value - k0) % y_new * z2, axis=0
+        )
+        if k0 < y_new - small:
+            extra = lax.ppermute(extra, axis_name=chip_axis, perm=all_rows)
+            local_now = lax.dynamic_update_slice_in_dim(
+                local_now, extra, (current_value + k0) % y_new * z2, axis=0
+            )
+    return local_now
+
+
+play_spans = functools.partial(settle_array_by_axis, chip_axis="tp")
 
 
 def with_halo(x, axis):
@@ -72,7 +99,7 @@
     for k in range(2):
         group = outgoing[:, k * 4 : (k + 1) * 4]
         arrived = lax.all_to_all(group, "sp", split_axis=0, concat_axis=0, tiled=True)
-        rows = lax.all_gather(arrived.reshape(-1, width), "tp", axis=0, tiled=True)
+        rows = play_spans(arrived.reshape(-1, width))
         gate_pre = jnp.dot(rows, gate_w[0], preferred_element_type=jnp.float32)
         up_pre = jnp.dot(rows, up_w[0], preferred_element_type=jnp.float32)
         active = clamped_unit(gate_pre, up_pre).astype(jnp.bfloat16)

time: 368 us -> 391 us (1.062)
  local copies, waits for them, and re-layouts: 14.8 us -> 25.9 us
  waiting for transfers between devices: 177 us -> 185 us
  starting transfers between devices: 33 us -> 39.5 us
  matrix products: 49.1 us -> 43.4 us
    ppermute x0 -> x6, waiting for transfers between devices: none -> 92.3 us  [the longest x4 92.3 us: settle_array_by_axis(): side_arr = lax.ppermute(side_arr, axis_name=chip_axis, perm=store)]
    all_gather x2 -> x0, waiting for transfers between devices: 46 us -> none  [local(): rows = lax.all_gather(arrived.reshape(-1, width), 'tp', axis=0, tiled=True)]
    reduce_scatter x2, waiting for transfers between devices: 74.2 us -> 35.4 us  [local(): lax.psum_scatter(partial.astype(jnp.bfloat16), 'tp', scatter_dimension=0,...]
    dot_general x2, matrix products: 13.1 us -> 7.38 us  [local(): up_pre = jnp.dot(rows, up_w[0], preferred_element_type=jnp.float32)]
    ppermute x0 -> x6, starting transfers between devices: none -> 5.51 us  [the longest x2 5.13 us: settle_array_by_axis(): extra = lax.ppermute(extra, axis_name=chip_axis, perm=all_rows)]
    unnamed x25 -> x35, local copies, waits for them, and re-layouts: 2.29 us -> 7.38 us
    dynamic_update_slice x0 -> x8, local copies, waits for them, and re-layouts: none -> 4.69 us  [the longest x4 2.86 us: settle_array_by_axis(): lax.dynamic_update_slice_in_dim(local_now, side_arr, (current_value - k0)...]
  transfers between devices with their start and end apart: 9 -> 13, of which waited for: 7 -> 8; matrix products, arithmetic and copies ran while one was open for 14% -> 9% of each run, Pallas kernels for 0% -> 0%
where the time goes in v1:
time: 391 us; the launch traced here: 390 us
  waiting for transfers between devices  185 us (47%)
  blocking collectives  77.8 us (20%)
  matrix products  43.4 us (11%)
  starting transfers between devices  39.5 us (10%)
  local copies, waits for them, and re-layouts  25.9 us (7%)
  between operations  13.8 us (4%)
  other arithmetic  4.81 us (1%)
    ppermute x4, waiting for transfers between devices, settle_array_by_axis(): side_arr = lax.ppermute(side_arr, axis_name=chip_axis, perm=store)  92.3 us
    all_to_all x2, blocking collectives, local(): lax.all_to_all(group, 'sp', split_axis=0, concat_axis=0, tiled=True)  77.8 us
    all_to_all x1, waiting for transfers between devices, local(): branch = lax.all_to_all(part, 'tp', split_axis=0, concat_axis=0, tiled=True)  35.6 us
    reduce_scatter x2, waiting for transfers between devices, local(): lax.psum_scatter(partial.astype(jnp.bfloat16), 'tp', scatter_dimension=0,...  35.4 us
    all_to_all x2, starting transfers between devices, local(): lax.all_to_all(summed.reshape(experts, 4, width), 'sp', split_axis=0, con...  22.7 us
    dot_general x2, matrix products, local(): partial = jnp.dot(active, down_w[0], preferred_element_type=jnp.float32)  20.6 us
    all_to_all x2, waiting for transfers between devices, local(): lax.all_to_all(summed.reshape(experts, 4, width), 'sp', split_axis=0, con...  19.3 us
  transfers between devices with their start and end apart: 13, of which 8 were waited for; matrix products, arithmetic and copies ran while one was open for 9% of the time, Pallas kernels for 0%

profile of v1, /device:TPU:1, one launch (start us, length us, event | category | flops | bytes accessed | tf_op | source)
XLA Modules:
  0.0 390.0 jit_solution(16133048525588361562)
XLA Ops:
  6.5 1.4 multiply_convert_fusion.2
  7.9 4.5 %collective-permute-start = (bf16[1,256]{1,0:T(2,128)(2,1)S(1)}, bf16[1,256]{1,0:T(2,128)(2,1)S(1)}, u32[]{:S(2)}, u32[]{:S(2)}) collective-permute-start(bf16[1,256]{1,0:T(2,128)(2,1)S(1)} %get-tuple-element.11), channel_id=1, source_target_pairs={{0,4},{4,8},{8,12},{12,16},{16,20},{20,24},{24,28},{28,32},{32,36}... | collective-permute-start | bytes 1544 | tf_op jit(solution)/shard_map/ppermute | solution.py:43
  12.4 1.9 collective-permute-start.1
  14.4 0.8 fusion.57
  15.2 2.2 collective-permute-done.1
  17.4 2.8 convolution_convert_fusion.2
  20.2 4.8 %all-to-all-start = ((bf16[4,192,2048]{2,1,0:T(8,128)(2,1)}), bf16[4,192,2048]{2,1,0:T(8,128)(2,1)}, u32[]{:S(2)}, u32[]{:S(2)}) async-start(bf16[4,192,2048]{2,1,0:T(8,128)(2,1)} %bitcast.54), calls=%async_computation | async-start | bytes 6291456 | tf_op jit(solution)/shard_map/all_to_all | solution.py:75
  26.0 35.6 %all-to-all-done = bf16[4,192,2048]{2,1,0:T(8,128)(2,1)} async-done(((bf16[4,192,2048]{2,1,0:T(8,128)(2,1)}), bf16[4,192,2048]{2,1,0:T(8,128)(2,1)}, u32[]{:S(2)}, u32[]{:S(2)}) %all-to-all-start) | async-done | bytes 3145760 | tf_op jit(solution)/shard_map/all_to_all | solution.py:75
  61.5 2.7 convert_reduce_fusion
  64.3 0.3 fusion.20
  64.6 0.9 copy-done.3
  65.5 0.8 fusion
  66.3 2.1 fusion.54
  68.5 40.7 %all_to_all.25 = bf16[64,4,2048]{2,1,0:T(4,128)(2,1)} all-to-all(bf16[64,4,2048]{2,1,0:T(4,128)(2,1)S(1)} %get-tuple-element.8), channel_id=1, replica_groups=mesh['sp'=64,'tp'=4] {'sp'}, dimensions={0} | all-to-all | bytes 2097152 | tf_op jit(solution)/shard_map/all_to_all | solution.py:101
  109.2 1.3 reshape.55
  110.8 2.5 collective-permute-start.6
  113.3 22.2 %collective-permute-done.5 = bf16[256,2048]{1,0:T(8,128)(2,1)} collective-permute-done((bf16[256,2048]{1,0:T(8,128)(2,1)S(1)}, bf16[256,2048]{1,0:T(8,128)(2,1)}, u32[]{:S(2)}, u32[]{:S(2)}) %collective-permute-start.5) | collective-permute-done | bytes 1048608 | tf_op jit(solution)/shard_map/ppermute | solution.py:24
  135.5 0.5 broadcast.29.clone
  136.1 1.3 constant_dynamic-update-slice_fusion.2
  137.5 1.5 constant_dynamic-update-slice_fusion.1
  138.9 20.8 %collective-permute-done.7 = bf16[256,2048]{1,0:T(8,128)(2,1)} collective-permute-done((bf16[256,2048]{1,0:T(8,128)(2,1)}, bf16[256,2048]{1,0:T(8,128)(2,1)}, u32[]{:S(2)}, u32[]{:S(2)}) %collective-permute-start.7) | collective-permute-done | bytes 1048608 | tf_op jit(solution)/shard_map/ppermute | solution.py:24
  159.7 1.3 constant_dynamic-update-slice_fusion
  161.0 2.0 copy-done.7
  163.0 3.7 fusion.12
  166.7 10.3 %convolution_convert_fusion = bf16[1024,2048]{1,0:T(8,128)(2,1)} fusion(bf16[1,512,2048]{2,1,0:T(8,128)(2,1)S(1)} %copy-done, f32[1024,512]{1,0:T(8,128)} %fusion.12, bf16[1024,2048]{1,0:T(8,128)(2,1)} %copy-done.7, bf16[1,2048,512]{2,1,0:T(8,128)(2,1)} %param.21), kind=kOutput, calls=%fused_computation.1 | convolution fusion | flops 4302307328 | bytes 14680064 | tf_op jit(solution)/shard_map/dot_general | solution.py:106
  177.1 1.1 copy-done.8
  178.2 37.1 %all_to_all.26 = bf16[64,4,2048]{2,1,0:T(4,128)(2,1)} all-to-all(bf16[64,4,2048]{2,1,0:T(4,128)(2,1)S(1)} %copy-done.8), channel_id=1, replica_groups=mesh['sp'=64,'tp'=4] {'sp'}, dimensions={0} | all-to-all | bytes 2097152 | tf_op jit(solution)/shard_map/all_to_all | solution.py:101
  215.3 1.3 reshape.53
  216.8 2.7 collective-permute-start.3
  219.4 25.2 %collective-permute-done.2 = bf16[256,2048]{1,0:T(8,128)(2,1)S(1)} collective-permute-done((bf16[256,2048]{1,0:T(8,128)(2,1)S(1)}, bf16[256,2048]{1,0:T(8,128)(2,1)S(1)}, u32[]{:S(2)}, u32[]{:S(2)}) %collective-permute-start.2) | collective-permute-done | bytes 1048608 | tf_op jit(solution)/shard_map/ppermute | solution.py:24
  244.6 0.5 broadcast.29.clone.1
  245.6 24.1 %collective-permute-done.4 = bf16[256,2048]{1,0:T(8,128)(2,1)S(1)} collective-permute-done((bf16[256,2048]{1,0:T(8,128)(2,1)S(1)}, bf16[256,2048]{1,0:T(8,128)(2,1)S(1)}, u32[]{:S(2)}, u32[]{:S(2)}) %collective-permute-start.4) | collective-permute-done | bytes 1048608 | tf_op jit(solution)/shard_map/ppermute | solution.py:24
  269.8 2.0 copy-done.6
  271.8 3.7 fusion.14
  275.4 10.3 %convolution_convert_fusion.1 = bf16[1024,2048]{1,0:T(8,128)(2,1)} fusion(bf16[1,512,2048]{2,1,0:T(8,128)(2,1)S(1)} %copy-done, f32[1024,512]{1,0:T(8,128)} %fusion.14, bf16[1024,2048]{1,0:T(8,128)(2,1)} %copy-done.6, bf16[1,2048,512]{2,1,0:T(8,128)(2,1)} %param.21), kind=kOutput, calls=%fused_computation.2 | convolution fusion | flops 4302307328 | bytes 14680064 | tf_op jit(solution)/shard_map/dot_general | solution.py:106
  285.8 2.2 reshape.56
  288.1 12.0 %all-to-all-start.4 = ((bf16[64,4,2048]{2,1,0:T(4,128)(2,1)}), bf16[64,4,2048]{2,1,0:T(4,128)(2,1)S(1)}, u32[]{:S(2)}, u32[]{:S(2)}) async-start(bf16[64,4,2048]{2,1,0:T(4,128)(2,1)} %reshape.56), calls=%async_computation.6 | async-start | bytes 2097152 | tf_op jit(solution)/shard_map/all_to_all | solution.py:111
  300.1 35.4 %reduce-scatter.3.cloned.1.call-done = bf16[256,2048]{1,0:T(8,128)(2,1)} async-done(((bf16[1024,2048]{1,0:T(8,128)(2,1)}), bf16[256,2048]{1,0:T(8,128)(2,1)}) %reduce-scatter.3.cloned.1.call-update) | async-done | bytes 1048592 | tf_op jit(solution)/shard_map/reduce_scatter | solution.py:107
  335.5 2.2 reshape.54
  337.7 1.0 copy-done.1
  338.7 10.7 %all-to-all-start.2 = ((bf16[64,4,2048]{2,1,0:T(4,128)(2,1)}), bf16[64,4,2048]{2,1,0:T(4,128)(2,1)S(1)}, u32[]{:S(2)}, u32[]{:S(2)}) async-start(bf16[64,4,2048]{2,1,0:T(4,128)(2,1)} %reshape.54), calls=%async_computation.3 | async-start | bytes 2097152 | tf_op jit(solution)/shard_map/all_to_all | solution.py:111
  349.6 1.0 copy.48
  350.6 1.4 fusion.55
  352.0 3.8 convolution_bitcast_fusion.1
  355.8 2.5 convolution_bitcast_fusion
  358.3 19.3 %all-to-all-done.2 = bf16[64,4,2048]{2,1,0:T(4,128)(2,1)S(1)} async-done(((bf16[64,4,2048]{2,1,0:T(4,128)(2,1)}), bf16[64,4,2048]{2,1,0:T(4,128)(2,1)S(1)}, u32[]{:S(2)}, u32[]{:S(2)}) %all-to-all-start.2) | async-done | bytes 1048608 | tf_op jit(solution)/shard_map/all_to_all | solution.py:111
  377.6 1.4 convolution_bitcast_fusion.2
  379.3 3.9 fusion.5
  (59 shorter events, 2.6 us)
Async XLA Ops:
  6.5 160.2 %copy-start = (bf16[1,512,2048]{2,1,0:T(8,128)(2,1)S(1)}, bf16[1,512,2048]{2,1,0:T(8,128)(2,1)}, u32[]{:S(2)}) copy-start(bf16[1,512,2048]{2,1,0:T(8,128)(2,1)} %param.23) | copy-start | bytes 6291460
  6.5 10.9 %copy-start.11 = (bf16[768,256]{1,0:T(8,128)(2,1)S(1)}, bf16[768,256]{1,0:T(8,128)(2,1)}, u32[]{:S(2)}) copy-start(bf16[768,256]{1,0:T(8,128)(2,1)} %param.14) | copy-start | bytes 1179652
  6.5 10.9 %copy-start.9 = (bf16[256,2048]{1,0:T(8,128)(2,1)S(1)}, bf16[256,2048]{1,0:T(8,128)(2,1)}, u32[]{:S(2)}) copy-start(bf16[256,2048]{1,0:T(8,128)(2,1)} %param.16) | copy-start | bytes 3145732
  7.9 7.2 %collective-permute-start = (bf16[1,256]{1,0:T(2,128)(2,1)S(1)}, bf16[1,256]{1,0:T(2,128)(2,1)S(1)}, u32[]{:S(2)}, u32[]{:S(2)}) collective-permute-start(bf16[1,256]{1,0:T(2,128)(2,1)S(1)} %get-tuple-element.11), channel_id=1, source_target_pairs={{0,4},{4,8},{8,12},{12,16},{16,20},{20,24},{24,28},{28,32},{32,36}... | collective-permute-start | bytes 1544 | tf_op jit(solution)/shard_map/ppermute | solution.py:43
  12.4 4.9 %collective-permute-start.1 = (bf16[1,256]{1,0:T(2,128)(2,1)S(1)}, bf16[1,256]{1,0:T(2,128)(2,1)S(1)}, u32[]{:S(2)}, u32[]{:S(2)}) collective-permute-start(bf16[1,256]{1,0:T(2,128)(2,1)S(1)} %get-tuple-element.12), channel_id=1, source_target_pairs={{4,0},{8,4},{12,8},{16,12},{20,16},{24,20},{28,24},{32,28},{36,32}... | collective-permute-start | bytes 1544 | tf_op jit(solution)/shard_map/ppermute | solution.py:44
  20.2 4.8 %copy-start.13 = (s32[192,2]{0,1:T(2,128)S(1)}, s32[192,2]{0,1:T(2,128)}, u32[]{:S(2)}) copy-start(s32[192,2]{0,1:T(2,128)} %param.19) | copy-start | bytes 4612
  20.2 41.3 %all-to-all-start = ((bf16[4,192,2048]{2,1,0:T(8,128)(2,1)}), bf16[4,192,2048]{2,1,0:T(8,128)(2,1)}, u32[]{:S(2)}, u32[]{:S(2)}) async-start(bf16[4,192,2048]{2,1,0:T(8,128)(2,1)} %bitcast.54), calls=%async_computation | async-start | bytes 6291456 | tf_op jit(solution)/shard_map/all_to_all | solution.py:75
  25.0 260.8 %reduce-scatter.5.cloned.1.call-start = ((), (), s32[]{:S(2)}) async-start(), calls=%async_computation.8 | async-start | bytes 5242880 | tf_op jit(solution)/shard_map/reduce_scatter | solution.py:107
  26.0 38.3 %copy-start.10 = (bf16[192,2048]{1,0:T(8,128)(2,1)S(1)}, bf16[192,2048]{1,0:T(8,128)(2,1)}, u32[]{:S(2)}) copy-start(bf16[192,2048]{1,0:T(8,128)(2,1)} %param.17) | copy-start | bytes 2359300
  64.3 1.2 copy-start.12
  64.6 0.9 copy-start.3
  110.5 25.0 %collective-permute-start.5 = (bf16[256,2048]{1,0:T(8,128)(2,1)S(1)}, bf16[256,2048]{1,0:T(8,128)(2,1)}, u32[]{:S(2)}, u32[]{:S(2)}) collective-permute-start(bf16[256,2048]{1,0:T(8,128)(2,1)S(1)} %reshape.55), channel_id=1, source_target_pairs={{0,1},{1,2},{2,3},{3,0},{4,5},{5,6},{6,7},{7,4},{8,9},{9,10},{10,1... | collective-permute-start | bytes 3145736 | tf_op jit(solution)/shard_map/ppermute | solution.py:24
  110.8 26.7 %collective-permute-start.6 = (bf16[256,2048]{1,0:T(8,128)(2,1)S(1)}, bf16[256,2048]{1,0:T(8,128)(2,1)}, u32[]{:S(2)}, u32[]{:S(2)}) collective-permute-start(bf16[256,2048]{1,0:T(8,128)(2,1)S(1)} %reshape.55), channel_id=1, source_target_pairs={{0,3},{1,0},{2,1},{3,2},{4,7},{5,4},{6,5},{7,6},{8,11},{9,8},{10,9... | collective-permute-start | bytes 3145736 | tf_op jit(solution)/shard_map/ppermute | solution.py:29
  135.5 24.2 %collective-permute-start.7 = (bf16[256,2048]{1,0:T(8,128)(2,1)}, bf16[256,2048]{1,0:T(8,128)(2,1)}, u32[]{:S(2)}, u32[]{:S(2)}) collective-permute-start(bf16[256,2048]{1,0:T(8,128)(2,1)} %collective-permute-done.5), channel_id=1, source_target_pairs={{0,1},{1,2},{2,3},{3,0},{4,5},{5,6},{6,7},{7,4},{8,9},{9,10},{10,1... | collective-permute-start | bytes 3145736 | tf_op jit(solution)/shard_map/ppermute | solution.py:24
  137.4 25.6 %copy-start.15 = (bf16[1,2048,512]{2,1,0:T(8,128)(2,1)S(1)}, bf16[1,2048,512]{2,1,0:T(8,128)(2,1)}, u32[]{:S(2)}) copy-start(bf16[1,2048,512]{2,1,0:T(8,128)(2,1)} %param.22) | copy-start | bytes 6291460
  161.0 2.0 copy-start.7
  177.0 1.2 copy-start.8
  177.0 158.5 %reduce-scatter.3.cloned.1.call-start = ((), (), s32[]{:S(2)}) async-start(), calls=%async_computation.7 | async-start | bytes 5242880 | tf_op jit(solution)/shard_map/reduce_scatter | solution.py:107
  216.7 28.0 %collective-permute-start.2 = (bf16[256,2048]{1,0:T(8,128)(2,1)S(1)}, bf16[256,2048]{1,0:T(8,128)(2,1)S(1)}, u32[]{:S(2)}, u32[]{:S(2)}) collective-permute-start(bf16[256,2048]{1,0:T(8,128)(2,1)S(1)} %reshape.53), channel_id=1, source_target_pairs={{0,1},{1,2},{2,3},{3,0},{4,5},{5,6},{6,7},{7,4},{8,9},{9,10},{10,1... | collective-permute-start | bytes 3145736 | tf_op jit(solution)/shard_map/ppermute | solution.py:24
  216.8 28.7 %collective-permute-start.3 = (bf16[256,2048]{1,0:T(8,128)(2,1)S(1)}, bf16[256,2048]{1,0:T(8,128)(2,1)S(1)}, u32[]{:S(2)}, u32[]{:S(2)}) collective-permute-start(bf16[256,2048]{1,0:T(8,128)(2,1)S(1)} %reshape.53), channel_id=1, source_target_pairs={{0,3},{1,0},{2,1},{3,2},{4,7},{5,4},{6,5},{7,6},{8,11},{9,8},{10,9... | collective-permute-start | bytes 3145736 | tf_op jit(solution)/shard_map/ppermute | solution.py:29
  244.6 25.0 %collective-permute-start.4 = (bf16[256,2048]{1,0:T(8,128)(2,1)S(1)}, bf16[256,2048]{1,0:T(8,128)(2,1)S(1)}, u32[]{:S(2)}, u32[]{:S(2)}) collective-permute-start(bf16[256,2048]{1,0:T(8,128)(2,1)S(1)} %collective-permute-done.2), channel_id=1, source_target_pairs={{0,1},{1,2},{2,3},{3,0},{4,5},{5,6},{6,7},{7,4},{8,9},{9,10},{10,1... | collective-permute-start | bytes 3145736 | tf_op jit(solution)/shard_map/ppermute | solution.py:24
  245.4 26.4 %copy-start.16 = (bf16[1,2048,512]{2,1,0:T(8,128)(2,1)S(1)}, bf16[1,2048,512]{2,1,0:T(8,128)(2,1)}, u32[]{:S(2)}) copy-start(bf16[1,2048,512]{2,1,0:T(8,128)(2,1)} %param.22) | copy-start | bytes 6291460
  269.8 2.0 copy-start.6
  288.1 49.7 %all-to-all-start.4 = ((bf16[64,4,2048]{2,1,0:T(4,128)(2,1)}), bf16[64,4,2048]{2,1,0:T(4,128)(2,1)S(1)}, u32[]{:S(2)}, u32[]{:S(2)}) async-start(bf16[64,4,2048]{2,1,0:T(4,128)(2,1)} %reshape.56), calls=%async_computation.6 | async-start | bytes 2097152 | tf_op jit(solution)/shard_map/all_to_all | solution.py:111
  300.1 49.4 %copy-start.14 = (f32[192,2]{0,1:T(2,128)S(1)}, f32[192,2]{0,1:T(2,128)}, u32[]{:S(2)}) copy-start(f32[192,2]{0,1:T(2,128)} %param.20) | copy-start | bytes 4612
  337.7 1.0 copy-start.1
  338.7 38.9 %all-to-all-start.2 = ((bf16[64,4,2048]{2,1,0:T(4,128)(2,1)}), bf16[64,4,2048]{2,1,0:T(4,128)(2,1)S(1)}, u32[]{:S(2)}, u32[]{:S(2)}) async-start(bf16[64,4,2048]{2,1,0:T(4,128)(2,1)} %reshape.54), calls=%async_computation.3 | async-start | bytes 2097152 | tf_op jit(solution)/shard_map/all_to_all | solution.py:111
  350.6 5.2 %copy-start.2 = (bf16[64,4,2048]{2,1,0:T(4,128)(2,1)S(1)}, bf16[64,4,2048]{2,1,0:T(4,128)(2,1)}, u32[]{:S(2)}) copy-start(bf16[64,4,2048]{2,1,0:T(4,128)(2,1)} %copy-done.1) | copy-start | bytes 3145732
  377.6 1.4 copy-start.4
  377.6 1.7 copy-start.5
Sparse Core Ops, SparseCore 0:
  177.2 47.5 reduce-scatter.4
  285.9 49.5 reduce-scatter.2
